TPU v7x, 128 devices: a whole 4x4x4 slice. The times are simulated.
128 devices in a mesh: sp: 32 (over z, y, core), tp: 4 (over x).
Axes of the slice: x: 4, y: 4, z: 4, core: 2. Of those that a mesh axis runs over, the one named last changes fastest.
Arguments:
- residual_in: bfloat16 [16384, 2048], P('sp'), may hold values from -6 to 6
- queries_nope: bfloat16 [16384, 1024], P('sp', 'tp'), may hold values from -15 to 15
- queries_rope: bfloat16 [16384, 512], P('sp', 'tp'), may hold values from -400 to 400
- latents: bfloat16 [16384, 256], P('sp'), may hold values from -6 to 6
- rope_keys: bfloat16 [16384, 32], P('sp'), may hold values from -8 to 8
- latent_norm_gain: float32 [256], replicated, may hold values from 0.1 to 1.9
- key_up_weight: bfloat16 [256, 1024], P(None, 'tp'), may hold values from -0.375 to 0.375
- value_up_weight: bfloat16 [256, 1024], P(None, 'tp'), may hold values from -0.375 to 0.375
- w_out: bfloat16 [1024, 2048], P('tp'), may hold values from -0.59765625 to 0.59765625
- norm_gain: float32 [2048], replicated, may hold values from 0.1 to 1.9
- w_up: bfloat16 [2048, 8192], P('sp', 'tp'), may hold values from -0.125 to 0.125
- w_down: bfloat16 [8192, 2048], P('tp', 'sp'), may hold values from -0.0625 to 0.0625
Outputs:
- layer_out: bfloat16 [16384, 2048], P('sp', 'tp')
All inputs are finite; a program needn't handle non-finite values.
Results may differ from a plain program's by a relative error of at most 0.015.
Values may be sent and summed in bfloat16 or wider, within the bound.
No kernel may reach another device: no remote copies, remote signals or barrier semaphores. Data moves between devices by JAX's collectives and lax.ppermute only.
A program may use at most 128 MiB of HBM per device.

v0:
```python
import math

import jax
import jax.numpy as jnp
from jax import lax
from jax.sharding import PartitionSpec as P

UNROTATED_WIDTH = 64
ROPE = 32


rope_base = 10000.0
epsilon = 1e-06


def in_one_piece(arrays, axis, dim, along):
    widths = [a.shape[along] for a in arrays]
    both = jnp.concatenate(arrays, axis=along)
    out = lax.all_gather(both, axis, axis=dim, tiled=True)
    return tuple(jnp.split(out, [sum(widths[:k]) for k in range(1, len(widths))], axis=along))


def sent_to_all(x, axis):
    copies = jnp.broadcast_to(x, (lax.axis_size(axis), *x.shape))
    return lax.all_to_all(copies, axis, split_axis=0, concat_axis=0, tiled=True)


def taken_together(x, axis):
    return sent_to_all(x, axis).astype(jnp.float32).sum(axis=0)


def in_blocks(x, dim, count):
    dims = x.shape
    parts = x.reshape(*dims[:dim], count, dims[dim] // count, *dims[dim + 1 :])
    return jnp.moveaxis(parts, dim, 0)


def sent_and_summed(x, axis, dim):
    count = lax.axis_size(axis)
    parts = lax.all_to_all(in_blocks(x, dim, count), axis, 0, 0, tiled=True)
    return jnp.sum(parts.astype(jnp.float32), axis=0)


def rotate(vectors, phases):
    half_width = vectors.shape[-1] // 2
    first_half = vectors[..., :half_width]
    second_half = vectors[..., half_width:]
    cosine = jnp.cos(phases)
    sine = jnp.sin(phases)
    return jnp.concatenate(
        [first_half * cosine - second_half * sine, second_half * cosine + first_half * sine],
        axis=-1,
    )


def rope_phases(positions, width):
    inverse = 1.0 / rope_base ** (jnp.arange(0, width, 2, dtype=jnp.float32) / width)
    return positions.astype(jnp.float32)[:, None] * inverse[None, :]


def rms_scale(vectors, gain_vec):
    return (
        vectors
        * lax.rsqrt(jnp.mean(vectors * vectors, axis=-1, keepdims=True) + epsilon)
        * gain_vec
    )


def attend_block(carry, queries, key_nope, value_rows, key_rot):
    row_peak, denominator, accum = carry
    key_count = key_nope.shape[0]
    heads = queries.shape[1]
    key_all = jnp.concatenate(
        [key_nope, jnp.broadcast_to(key_rot[:, None, :], (key_count, heads, key_rot.shape[1]))],
        axis=2,
    )
    scores = jnp.einsum("qhd,khd->hqk", queries, key_all, preferred_element_type=jnp.float32) * (
        1.0 / math.sqrt(UNROTATED_WIDTH + ROPE)
    )
    new_peak = jnp.maximum(row_peak, jnp.max(scores, axis=2))
    factor = jnp.exp(row_peak - new_peak)
    weights = jnp.exp(scores - new_peak[:, :, None])
    denominator = denominator * factor + jnp.sum(weights, axis=2)
    accum = accum * jnp.transpose(factor)[:, :, None] + jnp.einsum(
        "hqk,khd->qhd", weights.astype(jnp.bfloat16), value_rows, preferred_element_type=jnp.float32
    )
    return (new_peak, denominator, accum)


def fold_blocks(carry, pieces, expand, queries):
    count = pieces[0].shape[0]
    width = math.gcd(count, 1024)

    def one_block(state, start):
        sliced = tuple((lax.dynamic_slice_in_dim(member, start, width, 0) for member in pieces))
        key_nope, value_rows, key_rot = expand(sliced)
        return attend_block(state, queries, key_nope, value_rows, key_rot)

    return lax.fori_loop(
        0, count // width, lambda turn, state: one_block(state, turn * width), carry
    )


def on_device(
    residual_in,
    queries_nope,
    queries_rope,
    latents,
    rope_keys,
    latent_norm_gain,
    key_up_weight,
    value_up_weight,
    w_out,
    norm_gain,
    w_up,
    w_down,
):
    whole_up = lax.all_gather(w_up, "sp", axis=0, tiled=True)
    whole_down = lax.all_gather(w_down, "sp", axis=1, tiled=True)
    rows = residual_in.shape[0]
    heads = key_up_weight.shape[1] // UNROTATED_WIDTH
    value_width = value_up_weight.shape[1] // heads
    positions = lax.axis_index("sp") * rows + jnp.arange(rows, dtype=jnp.int32)
    phases = rope_phases(positions, ROPE)
    q_rot = rotate(
        queries_rope.astype(jnp.float32).reshape(rows, heads, ROPE), phases[:, None, :]
    ).astype(jnp.bfloat16)
    queries = jnp.concatenate([queries_nope.reshape(rows, heads, UNROTATED_WIDTH), q_rot], axis=2)
    lat_norm = rms_scale(latents.astype(jnp.float32), latent_norm_gain).astype(jnp.bfloat16)
    key_rot = rotate(rope_keys.astype(jnp.float32), phases).astype(jnp.bfloat16)
    start_carry = (
        jnp.full((heads, rows), -1e30, jnp.float32),
        jnp.zeros((heads, rows), jnp.float32),
        jnp.zeros((rows, heads, value_width), jnp.float32),
    )

    def expand_latent(sliced):
        lat_rows, rot_rows = sliced
        count = lat_rows.shape[0]
        key_nope = (
            jnp.dot(lat_rows, key_up_weight, preferred_element_type=jnp.float32)
            .astype(jnp.bfloat16)
            .reshape(count, heads, UNROTATED_WIDTH)
        )
        value_rows = (
            jnp.dot(lat_rows, value_up_weight, preferred_element_type=jnp.float32)
            .astype(jnp.bfloat16)
            .reshape(count, heads, value_width)
        )
        return (key_nope, value_rows, rot_rows)

    result = fold_blocks(
        start_carry, in_one_piece((lat_norm, key_rot), "sp", 0, 1), expand_latent, queries
    )
    row_peak, denominator, accum = result
    attended = (
        (accum / jnp.transpose(denominator)[:, :, None])
        .astype(jnp.bfloat16)
        .reshape(rows, heads * value_width)
    )
    part_term = jnp.dot(attended, w_out, preferred_element_type=jnp.float32)
    summed = taken_together(part_term.astype(jnp.bfloat16), "tp").astype(jnp.float32)
    stream = residual_in.astype(jnp.float32) + summed
    normed = rms_scale(stream, norm_gain).astype(jnp.bfloat16)
    upward = jnp.dot(normed, whole_up, preferred_element_type=jnp.float32)
    hidden = jnp.square(jax.nn.relu(upward)).astype(jnp.bfloat16)
    terms = jnp.dot(hidden, whole_down, preferred_element_type=jnp.float32)
    mixer = sent_and_summed(terms.astype(jnp.bfloat16), "tp", 1)
    own_width = mixer.shape[1]
    own_stream = lax.dynamic_slice_in_dim(stream, lax.axis_index("tp") * own_width, own_width, 1)
    return (own_stream + mixer).astype(jnp.bfloat16)


def solution(mesh):
    in_specs = (
        P("sp", None),
        P("sp", "tp"),
        P("sp", "tp"),
        P("sp", None),
        P("sp", None),
        P(),
        P(None, "tp"),
        P(None, "tp"),
        P("tp", None),
        P(),
        P("sp", "tp"),
        P("tp", "sp"),
    )
    out_specs = P("sp", "tp")
    return jax.shard_map(
        on_device, mesh=mesh, in_specs=in_specs, out_specs=out_specs, check_vma=False
    )
```

profile of v0, /device:TPU:0, one launch (start us, length us, event | category | flops | bytes accessed | tf_op | source)
XLA Modules:
  0.0 482.4 jit_solution(14162691038724398245)
XLA Ops:
  14.1 60.4 %all-gather.4.cloned.1.call-done = bf16[16384,288]{0,1:T(8,128)(2,1)} async-done(((bf16[512,288]{0,1:T(8,128)(2,1)}), bf16[16384,288]{0,1:T(8,128)(2,1)}) %all-gather.4.cloned.1.call-update) | async-done | bytes 9437200 | tf_op jit(solution)/shard_map/all_gather | solution.py:19
  74.5 7.6 %split.8 = bf16[16384,256]{0,1:T(8,128)(2,1)} slice(bf16[16384,288]{0,1:T(8,128)(2,1)} %all-gather.4.cloned.1.call-done), slice={[0:16384], [0:256]} | slice | bytes 16777216 | tf_op jit(solution)/shard_map/split | solution.py:20
  82.1 235.9 %while.18 = (s32[]{:T(128)}, f32[4,512]{1,0:T(4,128)S(1)}, f32[4,512]{1,0:T(4,128)S(1)}, f32[512,4,64]{0,2,1:T(8,128)S(1)}, bf16[16384,256]{0,1:T(8,128)(2,1)}, ...) while((s32[]{:T(128)}, f32[4,512]{1,0:T(4,128)S(1)}, ...), condition=%wide.region_4.0_spmd.clone, body=%wide.region_1.0_spmd.clone.sunk | while | flops 958803968 | bytes 64422108 | solution.py:99
  82.2 1.4 convolution_convert_fusion.6
  83.6 4.5 bitcast_reduce_fusion.2
  88.2 1.4 convolution_convert_fusion.7
  89.6 5.2 %fusion.62 = f32[512,4,64]{0,2,1:T(8,128)S(1)} fusion(bf16[1024,4,64]{0,2,1:T(8,128)(2,1)S(1)} %bitcast.68, f32[4,1024,512]{2,1,0:T(8,128)} %get-tuple-element.312, f32[4,512]{1,0:T(4,128)S(1)} %get-tuple-element.341, f32[512,4,64]{0,2,1:T(8,128)S(1)} %get-tuple-element.330, f32[512,4]{0,1:T(4,128)S(1)} %get-tuple-element.313, pred[]{:T(512)S(6)} %compare.3), kind=kOutput, calls=%fused_computation.9.clone.1 | convolution fusion | flops 275120128 | bytes 9977857 | tf_op jit(solution)/shard_map/while/body/eval_jaxpr/hqk,khd->qhd/dot_general | solution.py:84
  96.8 1.4 convolution_convert_fusion.6
  98.3 4.5 bitcast_reduce_fusion.2
  102.9 1.4 convolution_convert_fusion.7
  104.3 5.3 %fusion.62 = f32[512,4,64]{0,2,1:T(8,128)S(1)} fusion(bf16[1024,4,64]{0,2,1:T(8,128)(2,1)S(1)} %bitcast.68, f32[4,1024,512]{2,1,0:T(8,128)} %get-tuple-element.312, f32[4,512]{1,0:T(4,128)S(1)} %get-tuple-element.341, f32[512,4,64]{0,2,1:T(8,128)S(1)} %get-tuple-element.330, f32[512,4]{0,1:T(4,128)S(1)} %get-tuple-element.313, pred[]{:T(512)S(6)} %compare.3), kind=kOutput, calls=%fused_computation.9.clone.1 | convolution fusion | flops 275120128 | bytes 9977857 | tf_op jit(solution)/shard_map/while/body/eval_jaxpr/hqk,khd->qhd/dot_general | solution.py:84
  113.6 4.5 bitcast_reduce_fusion.2
  118.1 1.4 convolution_convert_fusion.7
  119.5 5.5 %fusion.62 = f32[512,4,64]{0,2,1:T(8,128)S(1)} fusion(bf16[1024,4,64]{0,2,1:T(8,128)(2,1)S(1)} %bitcast.68, f32[4,1024,512]{2,1,0:T(8,128)} %get-tuple-element.312, f32[4,512]{1,0:T(4,128)S(1)} %get-tuple-element.341, f32[512,4,64]{0,2,1:T(8,128)S(1)} %get-tuple-element.330, f32[512,4]{0,1:T(4,128)S(1)} %get-tuple-element.313, pred[]{:T(512)S(6)} %compare.3), kind=kOutput, calls=%fused_computation.9.clone.1 | convolution fusion | flops 275120128 | bytes 9977857 | tf_op jit(solution)/shard_map/while/body/eval_jaxpr/hqk,khd->qhd/dot_general | solution.py:84
  127.3 1.4 convolution_convert_fusion.6
  128.8 4.5 bitcast_reduce_fusion.2
  133.4 1.4 convolution_convert_fusion.7
  134.7 5.1 %fusion.62 = f32[512,4,64]{0,2,1:T(8,128)S(1)} fusion(bf16[1024,4,64]{0,2,1:T(8,128)(2,1)S(1)} %bitcast.68, f32[4,1024,512]{2,1,0:T(8,128)} %get-tuple-element.312, f32[4,512]{1,0:T(4,128)S(1)} %get-tuple-element.341, f32[512,4,64]{0,2,1:T(8,128)S(1)} %get-tuple-element.330, f32[512,4]{0,1:T(4,128)S(1)} %get-tuple-element.313, pred[]{:T(512)S(6)} %compare.3), kind=kOutput, calls=%fused_computation.9.clone.1 | convolution fusion | flops 275120128 | bytes 9977857 | tf_op jit(solution)/shard_map/while/body/eval_jaxpr/hqk,khd->qhd/dot_general | solution.py:84
  143.4 4.5 bitcast_reduce_fusion.2
  148.0 1.4 convolution_convert_fusion.7
  149.4 5.2 %fusion.62 = f32[512,4,64]{0,2,1:T(8,128)S(1)} fusion(bf16[1024,4,64]{0,2,1:T(8,128)(2,1)S(1)} %bitcast.68, f32[4,1024,512]{2,1,0:T(8,128)} %get-tuple-element.312, f32[4,512]{1,0:T(4,128)S(1)} %get-tuple-element.341, f32[512,4,64]{0,2,1:T(8,128)S(1)} %get-tuple-element.330, f32[512,4]{0,1:T(4,128)S(1)} %get-tuple-element.313, pred[]{:T(512)S(6)} %compare.3), kind=kOutput, calls=%fused_computation.9.clone.1 | convolution fusion | flops 275120128 | bytes 9977857 | tf_op jit(solution)/shard_map/while/body/eval_jaxpr/hqk,khd->qhd/dot_general | solution.py:84
  156.6 1.4 convolution_convert_fusion.6
  158.1 4.8 bitcast_reduce_fusion.2
  162.9 1.4 convolution_convert_fusion.7
  164.3 5.1 %fusion.62 = f32[512,4,64]{0,2,1:T(8,128)S(1)} fusion(bf16[1024,4,64]{0,2,1:T(8,128)(2,1)S(1)} %bitcast.68, f32[4,1024,512]{2,1,0:T(8,128)} %get-tuple-element.312, f32[4,512]{1,0:T(4,128)S(1)} %get-tuple-element.341, f32[512,4,64]{0,2,1:T(8,128)S(1)} %get-tuple-element.330, f32[512,4]{0,1:T(4,128)S(1)} %get-tuple-element.313, pred[]{:T(512)S(6)} %compare.3), kind=kOutput, calls=%fused_computation.9.clone.1 | convolution fusion | flops 275120128 | bytes 9977857 | tf_op jit(solution)/shard_map/while/body/eval_jaxpr/hqk,khd->qhd/dot_general | solution.py:84
  171.8 1.5 convolution_convert_fusion.6
  173.3 4.5 bitcast_reduce_fusion.2
  177.9 1.4 convolution_convert_fusion.7
  179.3 5.3 %fusion.62 = f32[512,4,64]{0,2,1:T(8,128)S(1)} fusion(bf16[1024,4,64]{0,2,1:T(8,128)(2,1)S(1)} %bitcast.68, f32[4,1024,512]{2,1,0:T(8,128)} %get-tuple-element.312, f32[4,512]{1,0:T(4,128)S(1)} %get-tuple-element.341, f32[512,4,64]{0,2,1:T(8,128)S(1)} %get-tuple-element.330, f32[512,4]{0,1:T(4,128)S(1)} %get-tuple-element.313, pred[]{:T(512)S(6)} %compare.3), kind=kOutput, calls=%fused_computation.9.clone.1 | convolution fusion | flops 275120128 | bytes 9977857 | tf_op jit(solution)/shard_map/while/body/eval_jaxpr/hqk,khd->qhd/dot_general | solution.py:84
  188.2 4.5 bitcast_reduce_fusion.2
  192.7 1.4 convolution_convert_fusion.7
  194.1 5.1 %fusion.62 = f32[512,4,64]{0,2,1:T(8,128)S(1)} fusion(bf16[1024,4,64]{0,2,1:T(8,128)(2,1)S(1)} %bitcast.68, f32[4,1024,512]{2,1,0:T(8,128)} %get-tuple-element.312, f32[4,512]{1,0:T(4,128)S(1)} %get-tuple-element.341, f32[512,4,64]{0,2,1:T(8,128)S(1)} %get-tuple-element.330, f32[512,4]{0,1:T(4,128)S(1)} %get-tuple-element.313, pred[]{:T(512)S(6)} %compare.3), kind=kOutput, calls=%fused_computation.9.clone.1 | convolution fusion | flops 275120128 | bytes 9977857 | tf_op jit(solution)/shard_map/while/body/eval_jaxpr/hqk,khd->qhd/dot_general | solution.py:84
  202.8 4.5 bitcast_reduce_fusion.2
  207.3 1.4 convolution_convert_fusion.7
  208.7 5.1 %fusion.62 = f32[512,4,64]{0,2,1:T(8,128)S(1)} fusion(bf16[1024,4,64]{0,2,1:T(8,128)(2,1)S(1)} %bitcast.68, f32[4,1024,512]{2,1,0:T(8,128)} %get-tuple-element.312, f32[4,512]{1,0:T(4,128)S(1)} %get-tuple-element.341, f32[512,4,64]{0,2,1:T(8,128)S(1)} %get-tuple-element.330, f32[512,4]{0,1:T(4,128)S(1)} %get-tuple-element.313, pred[]{:T(512)S(6)} %compare.3), kind=kOutput, calls=%fused_computation.9.clone.1 | convolution fusion | flops 275120128 | bytes 9977857 | tf_op jit(solution)/shard_map/while/body/eval_jaxpr/hqk,khd->qhd/dot_general | solution.py:84
  217.3 4.5 bitcast_reduce_fusion.2
  221.9 1.4 convolution_convert_fusion.7
  223.3 5.1 %fusion.62 = f32[512,4,64]{0,2,1:T(8,128)S(1)} fusion(bf16[1024,4,64]{0,2,1:T(8,128)(2,1)S(1)} %bitcast.68, f32[4,1024,512]{2,1,0:T(8,128)} %get-tuple-element.312, f32[4,512]{1,0:T(4,128)S(1)} %get-tuple-element.341, f32[512,4,64]{0,2,1:T(8,128)S(1)} %get-tuple-element.330, f32[512,4]{0,1:T(4,128)S(1)} %get-tuple-element.313, pred[]{:T(512)S(6)} %compare.3), kind=kOutput, calls=%fused_computation.9.clone.1 | convolution fusion | flops 275120128 | bytes 9977857 | tf_op jit(solution)/shard_map/while/body/eval_jaxpr/hqk,khd->qhd/dot_general | solution.py:84
  231.9 4.5 bitcast_reduce_fusion.2
  236.5 1.4 convolution_convert_fusion.7
  237.9 5.1 %fusion.62 = f32[512,4,64]{0,2,1:T(8,128)S(1)} fusion(bf16[1024,4,64]{0,2,1:T(8,128)(2,1)S(1)} %bitcast.68, f32[4,1024,512]{2,1,0:T(8,128)} %get-tuple-element.312, f32[4,512]{1,0:T(4,128)S(1)} %get-tuple-element.341, f32[512,4,64]{0,2,1:T(8,128)S(1)} %get-tuple-element.330, f32[512,4]{0,1:T(4,128)S(1)} %get-tuple-element.313, pred[]{:T(512)S(6)} %compare.3), kind=kOutput, calls=%fused_computation.9.clone.1 | convolution fusion | flops 275120128 | bytes 9977857 | tf_op jit(solution)/shard_map/while/body/eval_jaxpr/hqk,khd->qhd/dot_general | solution.py:84
  246.5 4.5 bitcast_reduce_fusion.2
  251.1 1.4 convolution_convert_fusion.7
  252.5 5.1 %fusion.62 = f32[512,4,64]{0,2,1:T(8,128)S(1)} fusion(bf16[1024,4,64]{0,2,1:T(8,128)(2,1)S(1)} %bitcast.68, f32[4,1024,512]{2,1,0:T(8,128)} %get-tuple-element.312, f32[4,512]{1,0:T(4,128)S(1)} %get-tuple-element.341, f32[512,4,64]{0,2,1:T(8,128)S(1)} %get-tuple-element.330, f32[512,4]{0,1:T(4,128)S(1)} %get-tuple-element.313, pred[]{:T(512)S(6)} %compare.3), kind=kOutput, calls=%fused_computation.9.clone.1 | convolution fusion | flops 275120128 | bytes 9977857 | tf_op jit(solution)/shard_map/while/body/eval_jaxpr/hqk,khd->qhd/dot_general | solution.py:84
  261.1 4.5 bitcast_reduce_fusion.2
  265.7 1.4 convolution_convert_fusion.7
  267.1 5.1 %fusion.62 = f32[512,4,64]{0,2,1:T(8,128)S(1)} fusion(bf16[1024,4,64]{0,2,1:T(8,128)(2,1)S(1)} %bitcast.68, f32[4,1024,512]{2,1,0:T(8,128)} %get-tuple-element.312, f32[4,512]{1,0:T(4,128)S(1)} %get-tuple-element.341, f32[512,4,64]{0,2,1:T(8,128)S(1)} %get-tuple-element.330, f32[512,4]{0,1:T(4,128)S(1)} %get-tuple-element.313, pred[]{:T(512)S(6)} %compare.3), kind=kOutput, calls=%fused_computation.9.clone.1 | convolution fusion | flops 275120128 | bytes 9977857 | tf_op jit(solution)/shard_map/while/body/eval_jaxpr/hqk,khd->qhd/dot_general | solution.py:84
  275.7 4.5 bitcast_reduce_fusion.2
  280.3 1.4 convolution_convert_fusion.7
  281.7 5.1 %fusion.62 = f32[512,4,64]{0,2,1:T(8,128)S(1)} fusion(bf16[1024,4,64]{0,2,1:T(8,128)(2,1)S(1)} %bitcast.68, f32[4,1024,512]{2,1,0:T(8,128)} %get-tuple-element.312, f32[4,512]{1,0:T(4,128)S(1)} %get-tuple-element.341, f32[512,4,64]{0,2,1:T(8,128)S(1)} %get-tuple-element.330, f32[512,4]{0,1:T(4,128)S(1)} %get-tuple-element.313, pred[]{:T(512)S(6)} %compare.3), kind=kOutput, calls=%fused_computation.9.clone.1 | convolution fusion | flops 275120128 | bytes 9977857 | tf_op jit(solution)/shard_map/while/body/eval_jaxpr/hqk,khd->qhd/dot_general | solution.py:84
  290.3 4.5 bitcast_reduce_fusion.2
  294.9 1.4 convolution_convert_fusion.7
  296.3 5.1 %fusion.62 = f32[512,4,64]{0,2,1:T(8,128)S(1)} fusion(bf16[1024,4,64]{0,2,1:T(8,128)(2,1)S(1)} %bitcast.68, f32[4,1024,512]{2,1,0:T(8,128)} %get-tuple-element.312, f32[4,512]{1,0:T(4,128)S(1)} %get-tuple-element.341, f32[512,4,64]{0,2,1:T(8,128)S(1)} %get-tuple-element.330, f32[512,4]{0,1:T(4,128)S(1)} %get-tuple-element.313, pred[]{:T(512)S(6)} %compare.3), kind=kOutput, calls=%fused_computation.9.clone.1 | convolution fusion | flops 275120128 | bytes 9977857 | tf_op jit(solution)/shard_map/while/body/eval_jaxpr/hqk,khd->qhd/dot_general | solution.py:84
  304.9 4.5 bitcast_reduce_fusion.2
  309.4 1.4 convolution_convert_fusion.7
  310.8 5.1 %fusion.62 = f32[512,4,64]{0,2,1:T(8,128)S(1)} fusion(bf16[1024,4,64]{0,2,1:T(8,128)(2,1)S(1)} %bitcast.68, f32[4,1024,512]{2,1,0:T(8,128)} %get-tuple-element.312, f32[4,512]{1,0:T(4,128)S(1)} %get-tuple-element.341, f32[512,4,64]{0,2,1:T(8,128)S(1)} %get-tuple-element.330, f32[512,4]{0,1:T(4,128)S(1)} %get-tuple-element.313, pred[]{:T(512)S(6)} %compare.3), kind=kOutput, calls=%fused_computation.9.clone.1 | convolution fusion | flops 275120128 | bytes 9977857 | tf_op jit(solution)/shard_map/while/body/eval_jaxpr/hqk,khd->qhd/dot_general | solution.py:84
  319.9 98.3 %all_to_all.10 = bf16[4,512,2048]{2,1,0:T(8,128)(2,1)} all-to-all(bf16[4,512,2048]{2,1,0:T(8,128)(2,1)S(1)} %broadcast_in_dim.45), channel_id=1, replica_groups=mesh['sp'=32,'tp'=4] {'tp'}, dimensions={0} | all-to-all | bytes 16777216 | tf_op jit(solution)/shard_map/all_to_all | solution.py:25
  418.2 5.8 %convert_reduce_fusion = f32[512,2048]{1,0:T(8,128)S(1)} fusion(bf16[4,512,2048]{2,1,0:T(8,128)(2,1)} %all_to_all.10), kind=kLoop, calls=%fused_computation.27 | loop fusion | flops 7340032 | bytes 12582912 | tf_op jit(solution)/shard_map/reduce_sum | solution.py:29
  424.0 2.5 multiply_reduce_fusion
  426.5 15.8 %convolution_convert_fusion.3 = bf16[512,2048]{1,0:T(8,128)(2,1)S(1)} fusion(bf16[2048,2048]{0,1:T(8,128)(2,1)} %all-gather.8.cloned.1.call-done, bf16[2048,2048]{1,0:T(8,128)(2,1)} %all-gather.6.cloned.1.call-done, f32[512,2048]{1,0:T(8,128)} %get-tuple-element.240, f32[2048]{0:T(1024)S(1)} %copy-done.5, f32[512]{0:T(512)S(1)} %add_rsqrt_fusion), kind=kOutput, calls=%fused_computation.34 | convolution fusion | flops 8597274624 | bytes 23078912 | tf_op jit(solution)/shard_map/dot_general | solution.py:167
  442.4 1.5 copy.34
  443.9 3.6 all-to-all-start.1
  447.5 25.8 %all-to-all-done.1 = bf16[4,512,512]{2,1,0:T(8,128)(2,1)S(1)} async-done(((bf16[4,512,512]{2,1,0:T(8,128)(2,1)}), bf16[4,512,512]{2,1,0:T(8,128)(2,1)S(1)}, u32[]{:S(2)}, u32[]{:S(2)}) %all-to-all-start.1) | async-done | bytes 2097184 | tf_op jit(solution)/shard_map/all_to_all | solution.py:40
  473.7 2.2 add_convert_fusion
  (180 shorter events, 58.9 us)
Async XLA Ops:
  6.5 311.5 %copy-start = (bf16[256,2048]{1,0:T(8,128)(2,1)S(1)}, bf16[256,2048]{1,0:T(8,128)(2,1)}, u32[]{:S(2)}) copy-start(bf16[256,2048]{1,0:T(8,128)(2,1)} %param.22) | copy-start | bytes 3145732
  6.5 68.0 %all-gather.4.cloned.1.call-start = ((), (), s32[]{:S(2)}) async-start(), calls=%async_computation.2 | async-start | bytes 9732096 | tf_op jit(solution)/shard_map/all_gather | solution.py:19
  10.4 416.2 %all-gather.6.cloned.1.call-start = ((), (), s32[]{:S(2)}) async-start(), calls=%async_computation.3 | async-start | bytes 8650752 | tf_op jit(solution)/shard_map/all_gather | solution.py:118
  11.1 415.4 %all-gather.8.cloned.1.call-start = ((), (), s32[]{:S(2)}) async-start(), calls=%async_computation.4 | async-start | bytes 8650752 | tf_op jit(solution)/shard_map/all_gather | solution.py:119
  14.1 68.1 %copy-start.2 = (bf16[256,256]{1,0:T(8,128)(2,1)S(1)}, bf16[256,256]{1,0:T(8,128)(2,1)}, u32[]{:S(2)}) copy-start(bf16[256,256]{1,0:T(8,128)(2,1)} %param.20) | copy-start | bytes 393220
  14.1 68.0 %copy-start.3 = (bf16[256,256]{1,0:T(8,128)(2,1)S(1)}, bf16[256,256]{1,0:T(8,128)(2,1)}, u32[]{:S(2)}) copy-start(bf16[256,256]{1,0:T(8,128)(2,1)} %param.21) | copy-start | bytes 393220
  74.5 7.6 %slice-start = ((bf16[16384,288]{0,1:T(8,128)(2,1)}), bf16[16384,32]{0,1:T(8,128)(2,1)S(1)}, s32[]{:S(2)}) async-start(bf16[16384,288]{0,1:T(8,128)(2,1)} %all-gather.4.cloned.1.call-done), calls=%async_computation.5 | async-start | bytes 2097152 | tf_op jit(solution)/shard_map/split | solution.py:20
  89.5 5.9 %copy-start.1 = (f32[4,1024,512]{2,1,0:T(8,128)S(1)}, f32[4,1024,512]{2,1,0:T(8,128)}, u32[]{:S(2)}) copy-start(f32[4,1024,512]{2,1,0:T(8,128)} %get-tuple-element.312) | copy-start | bytes 25165828 | tf_op jit(solution)/shard_map/while
  104.3 6.5 %copy-start.1 = (f32[4,1024,512]{2,1,0:T(8,128)S(1)}, f32[4,1024,512]{2,1,0:T(8,128)}, u32[]{:S(2)}) copy-start(f32[4,1024,512]{2,1,0:T(8,128)} %get-tuple-element.312) | copy-start | bytes 25165828 | tf_op jit(solution)/shard_map/while
  119.5 6.4 %copy-start.1 = (f32[4,1024,512]{2,1,0:T(8,128)S(1)}, f32[4,1024,512]{2,1,0:T(8,128)}, u32[]{:S(2)}) copy-start(f32[4,1024,512]{2,1,0:T(8,128)} %get-tuple-element.312) | copy-start | bytes 25165828 | tf_op jit(solution)/shard_map/while
  134.7 5.8 %copy-start.1 = (f32[4,1024,512]{2,1,0:T(8,128)S(1)}, f32[4,1024,512]{2,1,0:T(8,128)}, u32[]{:S(2)}) copy-start(f32[4,1024,512]{2,1,0:T(8,128)} %get-tuple-element.312) | copy-start | bytes 25165828 | tf_op jit(solution)/shard_map/while
  149.3 5.8 %copy-start.1 = (f32[4,1024,512]{2,1,0:T(8,128)S(1)}, f32[4,1024,512]{2,1,0:T(8,128)}, u32[]{:S(2)}) copy-start(f32[4,1024,512]{2,1,0:T(8,128)} %get-tuple-element.312) | copy-start | bytes 25165828 | tf_op jit(solution)/shard_map/while
  164.3 6.1 %copy-start.1 = (f32[4,1024,512]{2,1,0:T(8,128)S(1)}, f32[4,1024,512]{2,1,0:T(8,128)}, u32[]{:S(2)}) copy-start(f32[4,1024,512]{2,1,0:T(8,128)} %get-tuple-element.312) | copy-start | bytes 25165828 | tf_op jit(solution)/shard_map/while
  179.3 6.0 %copy-start.1 = (f32[4,1024,512]{2,1,0:T(8,128)S(1)}, f32[4,1024,512]{2,1,0:T(8,128)}, u32[]{:S(2)}) copy-start(f32[4,1024,512]{2,1,0:T(8,128)} %get-tuple-element.312) | copy-start | bytes 25165828 | tf_op jit(solution)/shard_map/while
  194.1 5.8 %copy-start.1 = (f32[4,1024,512]{2,1,0:T(8,128)S(1)}, f32[4,1024,512]{2,1,0:T(8,128)}, u32[]{:S(2)}) copy-start(f32[4,1024,512]{2,1,0:T(8,128)} %get-tuple-element.312) | copy-start | bytes 25165828 | tf_op jit(solution)/shard_map/while
  208.7 5.8 %copy-start.1 = (f32[4,1024,512]{2,1,0:T(8,128)S(1)}, f32[4,1024,512]{2,1,0:T(8,128)}, u32[]{:S(2)}) copy-start(f32[4,1024,512]{2,1,0:T(8,128)} %get-tuple-element.312) | copy-start | bytes 25165828 | tf_op jit(solution)/shard_map/while
  223.3 5.8 %copy-start.1 = (f32[4,1024,512]{2,1,0:T(8,128)S(1)}, f32[4,1024,512]{2,1,0:T(8,128)}, u32[]{:S(2)}) copy-start(f32[4,1024,512]{2,1,0:T(8,128)} %get-tuple-element.312) | copy-start | bytes 25165828 | tf_op jit(solution)/shard_map/while
  237.9 5.8 %copy-start.1 = (f32[4,1024,512]{2,1,0:T(8,128)S(1)}, f32[4,1024,512]{2,1,0:T(8,128)}, u32[]{:S(2)}) copy-start(f32[4,1024,512]{2,1,0:T(8,128)} %get-tuple-element.312) | copy-start | bytes 25165828 | tf_op jit(solution)/shard_map/while
  252.5 5.8 %copy-start.1 = (f32[4,1024,512]{2,1,0:T(8,128)S(1)}, f32[4,1024,512]{2,1,0:T(8,128)}, u32[]{:S(2)}) copy-start(f32[4,1024,512]{2,1,0:T(8,128)} %get-tuple-element.312) | copy-start | bytes 25165828 | tf_op jit(solution)/shard_map/while
  267.1 5.8 %copy-start.1 = (f32[4,1024,512]{2,1,0:T(8,128)S(1)}, f32[4,1024,512]{2,1,0:T(8,128)}, u32[]{:S(2)}) copy-start(f32[4,1024,512]{2,1,0:T(8,128)} %get-tuple-element.312) | copy-start | bytes 25165828 | tf_op jit(solution)/shard_map/while
  281.7 5.8 %copy-start.1 = (f32[4,1024,512]{2,1,0:T(8,128)S(1)}, f32[4,1024,512]{2,1,0:T(8,128)}, u32[]{:S(2)}) copy-start(f32[4,1024,512]{2,1,0:T(8,128)} %get-tuple-element.312) | copy-start | bytes 25165828 | tf_op jit(solution)/shard_map/while
  296.2 5.8 %copy-start.1 = (f32[4,1024,512]{2,1,0:T(8,128)S(1)}, f32[4,1024,512]{2,1,0:T(8,128)}, u32[]{:S(2)}) copy-start(f32[4,1024,512]{2,1,0:T(8,128)} %get-tuple-element.312) | copy-start | bytes 25165828 | tf_op jit(solution)/shard_map/while
  310.8 5.8 %copy-start.1 = (f32[4,1024,512]{2,1,0:T(8,128)S(1)}, f32[4,1024,512]{2,1,0:T(8,128)}, u32[]{:S(2)}) copy-start(f32[4,1024,512]{2,1,0:T(8,128)} %get-tuple-element.312) | copy-start | bytes 25165828 | tf_op jit(solution)/shard_map/while
  418.2 5.8 %copy-start.4 = (bf16[512,2048]{1,0:T(8,128)(2,1)S(1)}, bf16[512,2048]{1,0:T(8,128)(2,1)}, u32[]{:S(2)}) copy-start(bf16[512,2048]{1,0:T(8,128)(2,1)} %param.14) | copy-start | bytes 6291460
  424.0 2.5 copy-start.5
  443.9 29.5 %all-to-all-start.1 = ((bf16[4,512,512]{2,1,0:T(8,128)(2,1)}), bf16[4,512,512]{2,1,0:T(8,128)(2,1)S(1)}, u32[]{:S(2)}, u32[]{:S(2)}) async-start(bf16[4,512,512]{2,1,0:T(8,128)(2,1)} %bitcast.70), calls=%async_computation.1 | async-start | bytes 4194304 | tf_op jit(solution)/shard_map/all_to_all | solution.py:40
Sparse Core Ops, SparseCore 0:
  10.5 64.0 all-gather.3
  76.8 52.4 all-gather.5
  131.6 52.3 all-gather.7
where the time goes:
time: 484 us; the launch traced here: 482 us
  matrix products  217 us (45%)
  blocking collectives  98.3 us (20%)
  waiting for transfers between devices  87.7 us (18%)
  other arithmetic  36.1 us (7%)
  local copies, waits for them, and re-layouts  25 us (5%)
  between operations  13.3 us (3%)
    all_to_all x1, blocking collectives, sent_to_all(): return lax.all_to_all(copies, axis, split_axis=0, concat_axis=0, tiled=True)  98.3 us
    dot_general x16, matrix products, attend_block(): jnp.einsum('hqk,khd->qhd', weights.astype(jnp.bfloat16), value_rows, pref...  83.2 us
    dot_general x16, matrix products, attend_block(): jnp.einsum('qhd,khd->hqk', queries, key_all, preferred_element_type=jnp.f...  73 us
    all_gather x1, waiting for transfers between devices, in_one_piece(): out = lax.all_gather(both, axis, axis=dim, tiled=True)  60.4 us
    all_to_all x1, waiting for transfers between devices, sent_and_summed(): parts = lax.all_to_all(in_blocks(x, dim, count), axis, 0, 0, tiled=True)  25.8 us
    dot_general x16, matrix products, expand_latent(): jnp.dot(lat_rows, key_up_weight, preferred_element_type=jnp.float32)  22.2 us
    dot_general x16, matrix products, expand_latent(): jnp.dot(lat_rows, value_up_weight, preferred_element_type=jnp.float32)  22.1 us
    reduce_sum x16, other arithmetic, attend_block(): denominator = denominator * factor + jnp.sum(weights, axis=2)  22 us
  transfers between devices with their start and end apart: 4, of which 2 were waited for; matrix products, arithmetic and copies ran while one was open for 50% of the time, Pallas kernels for 0%

commit v1 on v0

v1 whole, which is shorter than its diff:
```python
import functools
import math

import jax
import jax.numpy as jnp
from jax import lax
from jax.experimental import pallas as pl
from jax.experimental.pallas import tpu as pltpu
from jax.sharding import PartitionSpec as P

UNROTATED_WIDTH = 64
ROPE = 32
VALUE_WIDTH = 64
LANES = 128
ROPE_END = UNROTATED_WIDTH + ROPE
VALUE_ROWS = 80
HEADROOM = 8.0
SUBBLOCKS = 4

rope_base = 10000.0
epsilon = 1e-06
SCALE = math.log2(math.e) / math.sqrt(ROPE_END)


def rotate(vectors, phases):
    half_width = vectors.shape[-1] // 2
    first_half = vectors[..., :half_width]
    second_half = vectors[..., half_width:]
    cosine = jnp.cos(phases)
    sine = jnp.sin(phases)
    return jnp.concatenate(
        [first_half * cosine - second_half * sine, second_half * cosine + first_half * sine],
        axis=-1,
    )


def rope_phases(positions, width):
    inverse = 1.0 / rope_base ** (jnp.arange(0, width, 2, dtype=jnp.float32) / width)
    return positions.astype(jnp.float32)[:, None] * inverse[None, :]


def rms_scale(vectors, gain_vec):
    return (
        vectors
        * lax.rsqrt(jnp.mean(vectors * vectors, axis=-1, keepdims=True) + epsilon)
        * gain_vec
    )


def dot(a, b, dims):
    return lax.dot_general(a, b, (dims, ((), ())), preferred_element_type=jnp.float32)


def attention_kernel(
    tokens,
    packed,
    latent_ref,
    key_up_ref,
    value_up_ref,
    query_ref,
    out_ref,
    shifted_ref,
    offset_ref,
    total_ref,
    block_ref,
    key_ref,
    value_ref,
):
    step = pl.program_id(0)
    heads, _, rows = query_ref.shape
    pieces = latent_ref.shape[0]
    groups = latent_ref.shape[2] // ROPE
    per_tile = LANES // ROPE

    @pl.when(step == 0)
    def _():
        shifted_ref[...] = query_ref[...]
        offset_ref[...] = jnp.zeros_like(offset_ref)
        total_ref[...] = jnp.zeros_like(total_ref)
        ones = lax.broadcasted_iota(
            jnp.int32, (heads, VALUE_ROWS - VALUE_WIDTH, value_ref.shape[2]), 1
        )
        value_ref[:, VALUE_WIDTH:, :] = jnp.where(ones == 0, 1.0, 0.0).astype(jnp.bfloat16)

    lane = lax.broadcasted_iota(jnp.int32, (packed, LANES), 1)
    is_rope = (lane >= UNROTATED_WIDTH) & (lane < ROPE_END)
    fill = jnp.where((lane == ROPE_END) | (lane == ROPE_END + 1), 1.0, 0.0)
    for piece in range(pieces):
        latent = latent_ref[piece, :tokens, :]
        keys = dot(latent, key_up_ref[...], ((1,), (0,)))
        for group in range(groups):
            tile = group // per_tile
            turned = latent_ref[piece, tokens:, tile * LANES : (tile + 1) * LANES]
            turned = turned.astype(jnp.float32)
            shift = (UNROTATED_WIDTH - ROPE * (group % per_tile)) % LANES
            if shift:
                turned = pltpu.roll(turned, shift, 1)
            turned = jnp.where(is_rope, turned, fill)
            for head in range(heads):
                own = keys[group * packed : (group + 1) * packed, head * LANES : (head + 1) * LANES]
                begin = piece * tokens + group * packed
                key_ref[head, begin : begin + packed, :] = (own * SCALE + turned).astype(
                    jnp.bfloat16
                )
        values = dot(value_up_ref[...], latent, ((1,), (1,))).astype(jnp.bfloat16)
        for head in range(heads):
            value_ref[head, :VALUE_WIDTH, piece * tokens : (piece + 1) * tokens] = values[
                head * VALUE_WIDTH : (head + 1) * VALUE_WIDTH, :
            ]

    peaks = []
    for head in range(heads):
        scores = dot(key_ref[head], shifted_ref[head], ((1,), (0,)))
        peaks.append(jnp.max(scores, axis=0, keepdims=True))
        weights = jnp.exp2(scores).astype(jnp.bfloat16)
        block_ref[head] = dot(value_ref[head], weights, ((1,), (0,)))
    peak = functools.reduce(jnp.maximum, peaks)
    rescale = (jnp.max(peak) > HEADROOM) | (step == 0)

    @pl.when(jnp.logical_not(rescale))
    def _():
        for head in range(heads):
            total_ref[head] = total_ref[head] + block_ref[head]

    @pl.when(rescale)
    def _():
        def one_head(head, carry):
            scores = dot(key_ref[head], shifted_ref[head], ((1,), (0,)))
            rise = jnp.max(scores, axis=0, keepdims=True)
            rise = jnp.where(step == 0, rise, jnp.maximum(rise, 0.0))
            old = offset_ref[head, 0:1, :]
            wanted = old + rise
            high = wanted.astype(jnp.bfloat16).astype(jnp.float32)
            low = (wanted - high).astype(jnp.bfloat16).astype(jnp.float32)
            new = high + low
            offset_ref[head, 0:1, :] = new
            row = lax.broadcasted_iota(jnp.int32, (16, rows), 0)
            shifted_ref[head, ROPE_END : ROPE_END + 16, :] = jnp.where(
                row == 0, -high, jnp.where(row == 1, -low, 0.0)
            ).astype(jnp.bfloat16)
            scores = dot(key_ref[head], shifted_ref[head], ((1,), (0,)))
            weights = jnp.exp2(scores).astype(jnp.bfloat16)
            factor = jnp.where(step == 0, 0.0, jnp.exp2(jnp.minimum(old - new, 0.0)))
            total_ref[head] = total_ref[head] * factor + dot(
                value_ref[head], weights, ((1,), (0,))
            )
            return carry

        lax.fori_loop(0, heads, one_head, 0)

    @pl.when(step == pl.num_programs(0) - 1)
    def _():
        for head in range(heads):
            total = total_ref[head]
            out_ref[head * VALUE_WIDTH : (head + 1) * VALUE_WIDTH, :] = (
                total[:VALUE_WIDTH] / total[VALUE_WIDTH : VALUE_WIDTH + 1]
            ).astype(jnp.bfloat16)


def attend(gathered, key_up, value_up, queries, tokens):
    devices, height, width = gathered.shape
    heads, _, rows = queries.shape
    pieces = math.gcd(devices, SUBBLOCKS)
    block = pieces * tokens
    return pl.pallas_call(
        functools.partial(attention_kernel, tokens, height - tokens),
        grid=(devices // pieces,),
        in_specs=[
            pl.BlockSpec((pieces, height, width), lambda i: (i, 0, 0)),
            pl.BlockSpec(key_up.shape, lambda i: (0, 0)),
            pl.BlockSpec(value_up.shape, lambda i: (0, 0)),
            pl.BlockSpec(queries.shape, lambda i: (0, 0, 0)),
        ],
        out_specs=pl.BlockSpec((heads * VALUE_WIDTH, rows), lambda i: (0, 0)),
        out_shape=jax.ShapeDtypeStruct((heads * VALUE_WIDTH, rows), jnp.bfloat16),
        scratch_shapes=[
            pltpu.VMEM(queries.shape, jnp.bfloat16),
            pltpu.VMEM((heads, 8, rows), jnp.float32),
            pltpu.VMEM((heads, VALUE_ROWS, rows), jnp.float32),
            pltpu.VMEM((heads, VALUE_ROWS, rows), jnp.float32),
            pltpu.VMEM((heads, block, LANES), jnp.bfloat16),
            pltpu.VMEM((heads, VALUE_ROWS, block), jnp.bfloat16),
        ],
        compiler_params=pltpu.CompilerParams(
            dimension_semantics=("arbitrary",), vmem_limit_bytes=50 * 1024 * 1024
        ),
        cost_estimate=pl.CostEstimate(
            flops=2 * heads * rows * devices * tokens * (LANES + VALUE_ROWS),
            bytes_accessed=gathered.size * 2,
            transcendentals=heads * rows * devices * tokens,
        ),
        name="attention",
    )(gathered, key_up, value_up, queries)


def in_blocks(x, dim, count):
    dims = x.shape
    parts = x.reshape(*dims[:dim], count, dims[dim] // count, *dims[dim + 1 :])
    return jnp.moveaxis(parts, dim, 0)


def sent_and_summed(x, axis, dim):
    count = lax.axis_size(axis)
    parts = lax.all_to_all(in_blocks(x, dim, count), axis, 0, 0, tiled=True)
    return jnp.sum(parts.astype(jnp.float32), axis=0)


def from_others(x, axis):
    count = lax.axis_size(axis)
    shifts = sorted(range(1, count), key=lambda k: -min(k, count - k))
    return {0: x} | {
        k: lax.ppermute(x, axis, [(i, (i + k) % count) for i in range(count)]) for k in shifts
    }


def on_device(
    residual_in,
    queries_nope,
    queries_rope,
    latents,
    rope_keys,
    latent_norm_gain,
    key_up_weight,
    value_up_weight,
    w_out,
    norm_gain,
    w_up,
    w_down,
):
    rows = residual_in.shape[0]
    heads = key_up_weight.shape[1] // UNROTATED_WIDTH
    latent_width = latents.shape[1]
    positions = lax.axis_index("sp") * rows + jnp.arange(rows, dtype=jnp.int32)
    phases = rope_phases(positions, ROPE)
    lat_norm = rms_scale(latents.astype(jnp.float32), latent_norm_gain).astype(jnp.bfloat16)
    key_rot = (rotate(rope_keys.astype(jnp.float32), phases) * SCALE).astype(jnp.bfloat16)
    groups = latent_width // ROPE
    packed = rows // groups
    key_rot = jnp.moveaxis(key_rot.reshape(groups, packed, ROPE), 0, 1)
    sent = jnp.concatenate([lat_norm, key_rot.reshape(packed, latent_width)], axis=0)
    gathered = lax.all_gather(sent, "sp", axis=0, tiled=False)

    whole_up = lax.all_gather(w_up, "sp", axis=0, tiled=True)
    whole_down = lax.all_gather(w_down, "sp", axis=1, tiled=True)
    out_parts = from_others(w_out, "tp")

    q_rot = rotate(
        queries_rope.astype(jnp.float32).reshape(rows, heads, ROPE), phases[:, None, :]
    ).astype(jnp.bfloat16)
    queries = jnp.concatenate(
        [
            queries_nope.reshape(rows, heads, UNROTATED_WIDTH),
            q_rot,
            jnp.zeros((rows, heads, LANES - ROPE_END), jnp.bfloat16),
        ],
        axis=2,
    )
    queries = jnp.transpose(queries, (1, 2, 0))
    key_up = jnp.pad(
        key_up_weight.reshape(latent_width, heads, UNROTATED_WIDTH),
        ((0, 0), (0, 0), (0, LANES - UNROTATED_WIDTH)),
    ).reshape(latent_width, heads * LANES)
    attended = attend(gathered, key_up, value_up_weight.T, queries, rows)

    parts = from_others(attended, "tp")
    stream = residual_in.astype(jnp.float32)
    for k in parts:
        stream = stream + dot(parts[k], out_parts[k], ((0,), (0,)))
    normed = rms_scale(stream, norm_gain).astype(jnp.bfloat16)
    upward = jnp.dot(normed, whole_up, preferred_element_type=jnp.float32)
    hidden = jnp.square(jax.nn.relu(upward)).astype(jnp.bfloat16)
    terms = jnp.dot(hidden, whole_down, preferred_element_type=jnp.float32)
    mixer = sent_and_summed(terms.astype(jnp.bfloat16), "tp", 1)
    own_width = mixer.shape[1]
    own_stream = lax.dynamic_slice_in_dim(stream, lax.axis_index("tp") * own_width, own_width, 1)
    return (own_stream + mixer).astype(jnp.bfloat16)


def solution(mesh):
    in_specs = (
        P("sp", None),
        P("sp", "tp"),
        P("sp", "tp"),
        P("sp", None),
        P("sp", None),
        P(),
        P(None, "tp"),
        P(None, "tp"),
        P("tp", None),
        P(),
        P("sp", "tp"),
        P("tp", "sp"),
    )
    out_specs = P("sp", "tp")
    return jax.shard_map(
        on_device, mesh=mesh, in_specs=in_specs, out_specs=out_specs, check_vma=False
    )
```

time: 484 us -> 238 us (0.49)
  matrix products: 217 us -> 22.7 us
  blocking collectives: 98.3 us -> 0 us
  Pallas kernels: 0 us -> 52.9 us
  other arithmetic: 36.1 us -> 6.66 us
  waiting for transfers between devices: 87.7 us -> 112 us
  local copies, waits for them, and re-layouts: 25 us -> 4.37 us
  starting transfers between devices: 3.69 us -> 24.2 us
    dot_general x65 -> x4, matrix products: 201 us -> 6.84 us  [dot(): lax.dot_general(a, b, (dims, ((), ())), preferred_element_type=jnp.float32)]
    all_to_all x1 -> x0, blocking collectives: 98.3 us -> none  [sent_to_all(): return lax.all_to_all(copies, axis, split_axis=0, concat_axis=0, tiled=True)]
    pallas_call x0 -> x1, Pallas kernels: none -> 52.9 us  [attend(): pl.pallas_call(functools.partial(attention_kernel, tokens, height - token...]
    all_gather x1, waiting for transfers between devices: 0.01 us -> 33.5 us  [on_device(): whole_down = lax.all_gather(w_down, 'sp', axis=1, tiled=True)]
    reduce_sum x17 -> x0, other arithmetic: 27.8 us -> none  [the longest x16 22 us: attend_block(): denominator = denominator * factor + jnp.sum(weights, axis=2)]
    ppermute x0 -> x6, starting transfers between devices: none -> 19.9 us  [from_others(): lax.ppermute(x, axis, [(i, (i + k) % count) for i in range(count)])]
    all_gather x1, waiting for transfers between devices: 60.4 us -> 47.2 us  [on_device(): gathered = lax.all_gather(sent, 'sp', axis=0, tiled=False)]
    while x48 -> x0, local copies, waits for them, and re-layouts: 11 us -> none
  transfers between devices with their start and end apart: 4 -> 10, of which waited for: 2 -> 5; matrix products, arithmetic and copies ran while one was open for 50% -> 4% of each run, Pallas kernels for 0% -> 22%
where the time goes in v1:
time: 238 us; the launch traced here: 236 us
  waiting for transfers between devices  112 us (47%)
  Pallas kernels  52.9 us (22%)
  starting transfers between devices  24.2 us (10%)
  matrix products  22.7 us (10%)
  between operations  13.3 us (6%)
  other arithmetic  6.66 us (3%)
  local copies, waits for them, and re-layouts  4.37 us (2%)
    pallas_call x1, Pallas kernels, attend(): pl.pallas_call(functools.partial(attention_kernel, tokens, height - token...  52.9 us
    all_gather x1, waiting for transfers between devices, on_device(): gathered = lax.all_gather(sent, 'sp', axis=0, tiled=False)  47.2 us
    all_gather x1, waiting for transfers between devices, on_device(): whole_down = lax.all_gather(w_down, 'sp', axis=1, tiled=True)  33.5 us
    all_to_all x1, waiting for transfers between devices, sent_and_summed(): parts = lax.all_to_all(in_blocks(x, dim, count), axis, 0, 0, tiled=True)  26.7 us
    ppermute x6, starting transfers between devices, from_others(): lax.ppermute(x, axis, [(i, (i + k) % count) for i in range(count)])  19.9 us
    dot_general x1, matrix products, on_device(): terms = jnp.dot(hidden, whole_down, preferred_element_type=jnp.float32)  15.8 us
    dot_general x4, matrix products, dot(): lax.dot_general(a, b, (dims, ((), ())), preferred_element_type=jnp.float32)  6.84 us
  transfers between devices with their start and end apart: 10, of which 5 were waited for; matrix products, arithmetic and copies ran while one was open for 4% of the time, Pallas kernels for 22%

profile of v1, /device:TPU:0, one launch (start us, length us, event | category | flops | bytes accessed | tf_op | source)
XLA Modules:
  0.0 235.6 jit_solution(2590683466409054530)
XLA Ops:
  6.5 0.0 copy-start.2
  6.5 0.0 copy-start.3
  6.5 0.0 all-gather.9.cloned.1.call-start
  6.6 0.8 convert_element_type.45
  7.4 0.2 multiply_cosine_fusion
  7.6 0.1 concatenate.17
  7.7 0.1 concatenate.18
  7.8 0.1 copy.27
  7.9 1.1 fusion.2
  9.0 1.1 fusion.4
  10.1 0.7 pad_maximum_fusion
  10.9 0.0 all-gather.9.cloned.1.call-update
  10.9 0.0 all-gather.5.cloned.1.call-start
  10.9 0.7 all-gather.5.cloned.1.call-update
  11.6 0.0 all-gather.7.cloned.1.call-start
  11.7 0.7 all-gather.7.cloned.1.call-update
  12.4 3.2 %collective-permute-start.1 = (bf16[256,2048]{1,0:T(8,128)(2,1)}, bf16[256,2048]{1,0:T(8,128)(2,1)S(1)}, u32[]{:S(2)}, u32[]{:S(2)}) collective-permute-start(bf16[256,2048]{1,0:T(8,128)(2,1)} %param.20), channel_id=1, source_target_pairs={{0,2},{1,3},{2,0},{3,1},{4,6},{5,7},{6,4},{7,5},{8,10},{9,11},{10,... | collective-permute-start | bytes 3145736 | tf_op jit(solution)/shard_map/ppermute | solution.py:212
  15.6 0.6 collective-permute-start.3
  16.2 2.6 %collective-permute-start.5 = (bf16[256,2048]{1,0:T(8,128)(2,1)}, bf16[256,2048]{1,0:T(8,128)(2,1)}, u32[]{:S(2)}, u32[]{:S(2)}) collective-permute-start(bf16[256,2048]{1,0:T(8,128)(2,1)} %param.20), channel_id=1, source_target_pairs={{0,3},{1,0},{2,1},{3,2},{4,7},{5,4},{6,5},{7,6},{8,11},{9,8},{10,9... | collective-permute-start | bytes 3145736 | tf_op jit(solution)/shard_map/ppermute | solution.py:212
  18.8 1.0 copy.32
  19.8 1.1 copy.31
  20.9 0.0 copy-done.2
  20.9 0.1 copy.28
  21.1 0.1 copy.34.key_up_ref
  21.2 0.0 copy-done.3
  21.2 0.1 copy.30
  21.4 0.1 pad.8.clone
  21.5 0.1 maximum_bitcast_fusion.query_ref
  21.6 47.2 %all-gather.9.cloned.1.call-done = bf16[18432,256]{1,0:T(8,128)(2,1)} async-done(((bf16[576,256]{1,0:T(8,128)(2,1)}), bf16[18432,256]{1,0:T(8,128)(2,1)}) %all-gather.9.cloned.1.call-update) | async-done | bytes 9437200 | tf_op jit(solution)/shard_map/all_gather | solution.py:241
  68.8 0.0 copy-start.1
  68.8 52.9 %attention.1 = bf16[256,512]{1,0:T(8,128)(2,1)S(1)} custom-call(bf16[32,576,256]{2,1,0:T(8,128)(2,1)} %bitcast.45, bf16[256,512]{1,0:T(8,128)(2,1)S(1)} %copy.34.key_up_ref, bf16[256,256]{1,0:T(8,128)(2,1)S(1)} %bitcast.37, bf16[4,128,512]{2,1,0:T(8,128)(2,1)S(1)} %maximum_bitcast_fusion.query_ref), custom_call_target="tpu_custom_call" | custom-call | flops 13958643712 | bytes 9437184 | tf_op jit(solution)/shard_map/attention/pallas_call | solution.py:165
  121.7 10.0 %collective-permute-start = (bf16[256,512]{1,0:T(8,128)(2,1)S(1)}, bf16[256,512]{1,0:T(8,128)(2,1)S(1)}, u32[]{:S(2)}, u32[]{:S(2)}) collective-permute-start(bf16[256,512]{1,0:T(8,128)(2,1)S(1)} %attention.1), channel_id=1, source_target_pairs={{0,2},{1,3},{2,0},{3,1},{4,6},{5,7},{6,4},{7,5},{8,10},{9,11},{10,... | collective-permute-start | bytes 786440 | tf_op jit(solution)/shard_map/ppermute | solution.py:212
  131.7 0.0 collective-permute-start.2
  131.7 0.0 copy-done.1
  131.7 0.7 fusion.6
  132.4 0.0 collective-permute-done.1
  132.4 3.5 %collective-permute-start.4 = (bf16[256,512]{1,0:T(8,128)(2,1)S(1)}, bf16[256,512]{1,0:T(8,128)(2,1)S(1)}, u32[]{:S(2)}, u32[]{:S(2)}) collective-permute-start(bf16[256,512]{1,0:T(8,128)(2,1)S(1)} %attention.1), channel_id=1, source_target_pairs={{0,3},{1,0},{2,1},{3,2},{4,7},{5,4},{6,5},{7,6},{8,11},{9,8},{10,9... | collective-permute-start | bytes 786440 | tf_op jit(solution)/shard_map/ppermute | solution.py:212
  135.9 0.1 collective-permute-done
  136.0 0.7 fusion.7
  136.7 0.0 copy-start
  136.8 0.0 collective-permute-done.3
  136.8 2.5 %collective-permute-done.2 = bf16[256,512]{1,0:T(8,128)(2,1)S(1)} collective-permute-done((bf16[256,512]{1,0:T(8,128)(2,1)S(1)}, bf16[256,512]{1,0:T(8,128)(2,1)S(1)}, u32[]{:S(2)}, u32[]{:S(2)}) %collective-permute-start.2) | collective-permute-done | bytes 262176 | tf_op jit(solution)/shard_map/ppermute | solution.py:212
  139.2 0.7 fusion.8
  140.0 0.0 copy-start.4
  140.0 0.0 collective-permute-done.5
  140.0 0.0 collective-permute-done.4
  140.0 0.0 copy-done
  140.0 4.6 %multiply_reduce_fusion = (f32[512]{0:T(512)S(1)}, f32[512,2048]{1,0:T(8,128)}) fusion(f32[512,2048]{1,0:T(8,128)S(1)} %fusion.8, f32[512,2048]{1,0:T(8,128)S(1)} %fusion.7, f32[512,2048]{1,0:T(8,128)S(1)} %fusion.6, bf16[512,2048]{1,0:T(8,128)(2,1)S(1)} %copy-done, bf16[256,512]{1,0:T(8,128)(2,1)S(1)} %collective-permute-done.4, ...), kind=kOutput, calls=%fused_computation.3 | convolution fusion | flops 544210432 | bytes 20187136 | tf_op jit(solution)/shard_map/dot_general | solution.py:51
  144.7 0.0 all-gather.5.cloned.1.call-done
  144.7 33.5 %all-gather.7.cloned.1.call-done = bf16[2048,2048]{0,1:T(8,128)(2,1)} async-done(((bf16[2048,64]{0,1:T(8,128)(2,1)}), bf16[2048,2048]{0,1:T(8,128)(2,1)}) %all-gather.7.cloned.1.call-update) | async-done | bytes 8388624 | tf_op jit(solution)/shard_map/all_gather | solution.py:244
  178.2 0.0 copy-done.4
  178.2 15.8 %convolution_convert_fusion = bf16[512,2048]{1,0:T(8,128)(2,1)S(1)} fusion(bf16[2048,2048]{0,1:T(8,128)(2,1)} %all-gather.7.cloned.1.call-done, bf16[2048,2048]{1,0:T(8,128)(2,1)} %all-gather.5.cloned.1.call-done, f32[512,2048]{1,0:T(8,128)} %get-tuple-element.6, f32[2048]{0:T(1024)S(1)} %copy-done.4, f32[512]{0:T(512)S(1)} %add_rsqrt_fusion), kind=kOutput, calls=%fused_computation.5 | convolution fusion | flops 8597274624 | bytes 23078912 | tf_op jit(solution)/shard_map/dot_general | solution.py:272
  194.0 1.5 copy.37
  195.6 4.3 %all-to-all-start = ((bf16[4,512,512]{2,1,0:T(8,128)(2,1)}), bf16[4,512,512]{2,1,0:T(8,128)(2,1)S(1)}, u32[]{:S(2)}, u32[]{:S(2)}) async-start(bf16[4,512,512]{2,1,0:T(8,128)(2,1)} %bitcast.38), calls=%async_computation | async-start | bytes 4194304 | tf_op jit(solution)/shard_map/all_to_all | solution.py:204
  199.8 26.7 %all-to-all-done = bf16[4,512,512]{2,1,0:T(8,128)(2,1)S(1)} async-done(((bf16[4,512,512]{2,1,0:T(8,128)(2,1)}), bf16[4,512,512]{2,1,0:T(8,128)(2,1)S(1)}, u32[]{:S(2)}, u32[]{:S(2)}) %all-to-all-start) | async-done | bytes 2097184 | tf_op jit(solution)/shard_map/all_to_all | solution.py:204
  226.6 0.3 convert_reduce_fusion
  226.9 2.2 add_convert_fusion
  (10 shorter events, 0.1 us)
Async XLA Ops:
  6.5 14.4 %copy-start.2 = (bf16[256,256]{1,0:T(8,128)(2,1)S(1)}, bf16[256,256]{1,0:T(8,128)(2,1)}, u32[]{:S(2)}) copy-start(bf16[256,256]{1,0:T(8,128)(2,1)} %param.18) | copy-start | bytes 393220
  6.5 14.7 %copy-start.3 = (bf16[256,256]{1,0:T(8,128)(2,1)S(1)}, bf16[256,256]{1,0:T(8,128)(2,1)}, u32[]{:S(2)}) copy-start(bf16[256,256]{1,0:T(8,128)(2,1)} %param.19) | copy-start | bytes 393220
  6.5 62.3 %all-gather.9.cloned.1.call-start = ((), (), s32[]{:S(2)}) async-start(), calls=%async_computation.3 | async-start | bytes 9732096 | tf_op jit(solution)/shard_map/all_gather | solution.py:241
  10.9 133.8 %all-gather.5.cloned.1.call-start = ((), (), s32[]{:S(2)}) async-start(), calls=%async_computation.1 | async-start | bytes 8650752 | tf_op jit(solution)/shard_map/all_gather | solution.py:243
  11.6 166.6 %all-gather.7.cloned.1.call-start = ((), (), s32[]{:S(2)}) async-start(), calls=%async_computation.2 | async-start | bytes 8650752 | tf_op jit(solution)/shard_map/all_gather | solution.py:244
  12.4 120.0 %collective-permute-start.1 = (bf16[256,2048]{1,0:T(8,128)(2,1)}, bf16[256,2048]{1,0:T(8,128)(2,1)S(1)}, u32[]{:S(2)}, u32[]{:S(2)}) collective-permute-start(bf16[256,2048]{1,0:T(8,128)(2,1)} %param.20), channel_id=1, source_target_pairs={{0,2},{1,3},{2,0},{3,1},{4,6},{5,7},{6,4},{7,5},{8,10},{9,11},{10,... | collective-permute-start | bytes 3145736 | tf_op jit(solution)/shard_map/ppermute | solution.py:212
  15.6 121.2 %collective-permute-start.3 = (bf16[256,2048]{1,0:T(8,128)(2,1)}, bf16[256,2048]{1,0:T(8,128)(2,1)S(1)}, u32[]{:S(2)}, u32[]{:S(2)}) collective-permute-start(bf16[256,2048]{1,0:T(8,128)(2,1)} %param.20), channel_id=1, source_target_pairs={{0,1},{1,2},{2,3},{3,0},{4,5},{5,6},{6,7},{7,4},{8,9},{9,10},{10,1... | collective-permute-start | bytes 3145736 | tf_op jit(solution)/shard_map/ppermute | solution.py:212
  16.2 123.8 %collective-permute-start.5 = (bf16[256,2048]{1,0:T(8,128)(2,1)}, bf16[256,2048]{1,0:T(8,128)(2,1)}, u32[]{:S(2)}, u32[]{:S(2)}) collective-permute-start(bf16[256,2048]{1,0:T(8,128)(2,1)} %param.20), channel_id=1, source_target_pairs={{0,3},{1,0},{2,1},{3,2},{4,7},{5,4},{6,5},{7,6},{8,11},{9,8},{10,9... | collective-permute-start | bytes 3145736 | tf_op jit(solution)/shard_map/ppermute | solution.py:212
  68.8 62.8 %copy-start.1 = (bf16[256,2048]{1,0:T(8,128)(2,1)S(1)}, bf16[256,2048]{1,0:T(8,128)(2,1)}, u32[]{:S(2)}) copy-start(bf16[256,2048]{1,0:T(8,128)(2,1)} %param.20) | copy-start | bytes 3145732
  121.7 14.3 %collective-permute-start = (bf16[256,512]{1,0:T(8,128)(2,1)S(1)}, bf16[256,512]{1,0:T(8,128)(2,1)S(1)}, u32[]{:S(2)}, u32[]{:S(2)}) collective-permute-start(bf16[256,512]{1,0:T(8,128)(2,1)S(1)} %attention.1), channel_id=1, source_target_pairs={{0,2},{1,3},{2,0},{3,1},{4,6},{5,7},{6,4},{7,5},{8,10},{9,11},{10,... | collective-permute-start | bytes 786440 | tf_op jit(solution)/shard_map/ppermute | solution.py:212
  131.7 7.6 %collective-permute-start.2 = (bf16[256,512]{1,0:T(8,128)(2,1)S(1)}, bf16[256,512]{1,0:T(8,128)(2,1)S(1)}, u32[]{:S(2)}, u32[]{:S(2)}) collective-permute-start(bf16[256,512]{1,0:T(8,128)(2,1)S(1)} %attention.1), channel_id=1, source_target_pairs={{0,1},{1,2},{2,3},{3,0},{4,5},{5,6},{6,7},{7,4},{8,9},{9,10},{10,1... | collective-permute-start | bytes 786440 | tf_op jit(solution)/shard_map/ppermute | solution.py:212
  132.4 7.6 %collective-permute-start.4 = (bf16[256,512]{1,0:T(8,128)(2,1)S(1)}, bf16[256,512]{1,0:T(8,128)(2,1)S(1)}, u32[]{:S(2)}, u32[]{:S(2)}) collective-permute-start(bf16[256,512]{1,0:T(8,128)(2,1)S(1)} %attention.1), channel_id=1, source_target_pairs={{0,3},{1,0},{2,1},{3,2},{4,7},{5,4},{6,5},{7,6},{8,11},{9,8},{10,9... | collective-permute-start | bytes 786440 | tf_op jit(solution)/shard_map/ppermute | solution.py:212
  136.7 3.3 %copy-start = (bf16[512,2048]{1,0:T(8,128)(2,1)S(1)}, bf16[512,2048]{1,0:T(8,128)(2,1)}, u32[]{:S(2)}) copy-start(bf16[512,2048]{1,0:T(8,128)(2,1)} %param.12) | copy-start | bytes 6291460
  140.0 38.2 %copy-start.4 = (f32[2048]{0:T(1024)S(1)}, f32[2048]{0:T(1024)}, u32[]{:S(2)}) copy-start(f32[2048]{0:T(1024)} %param.21) | copy-start | bytes 24580
  195.6 31.0 %all-to-all-start = ((bf16[4,512,512]{2,1,0:T(8,128)(2,1)}), bf16[4,512,512]{2,1,0:T(8,128)(2,1)S(1)}, u32[]{:S(2)}, u32[]{:S(2)}) async-start(bf16[4,512,512]{2,1,0:T(8,128)(2,1)} %bitcast.38), calls=%async_computation | async-start | bytes 4194304 | tf_op jit(solution)/shard_map/all_to_all | solution.py:204
Sparse Core Ops, SparseCore 0:
  11.0 57.7 all-gather.8
  71.1 52.3 all-gather.4
  125.8 52.3 all-gather.6
